TPU v7x, 32 devices: a whole 2x2x4 slice. The times are simulated.
32 devices in a mesh: ep: 8 (over z, x), tp: 4 (over y, core).
Axes of the slice: x: 2, y: 2, z: 4, core: 2. Of those that a mesh axis runs over, the one named last changes fastest.
Arguments:
- tokens: bfloat16 [1024, 2048], P('ep'), may hold values from -6 to 6
- norm_gain: float32 [2048], replicated, may hold values from 0.1 to 1.9
- expert_ids: int32 [1024, 2], P('ep'), may hold values from 0 to 7, all different within a row; in each aligned block of 128 rows (0 to 127, 128 to 255, ...) at most 64 rows name the same one
- route_weights: float32 [1024, 2], P('ep'), may hold values from 0.2 to 1
- w_gate: bfloat16 [8, 2048, 4096], P('ep', None, 'tp'), may hold values from -0.125 to 0.125
- w_up: bfloat16 [8, 2048, 4096], P('ep', None, 'tp'), may hold values from -0.125 to 0.125
- w_down: bfloat16 [8, 4096, 2048], P('ep', 'tp'), may hold values from -0.09375 to 0.09375
Outputs:
- combined: bfloat16 [1024, 2048], P('ep', 'tp')
Inputs may be any that keep to these rules, and one draw needn't show every extreme that they name: `expert_ids`: each row names two different experts; among the rows of one device no expert is named more than 64 times, and in every draw some expert is named exactly 64 times there.
All inputs are finite; a program needn't handle non-finite values.
Results may differ from a plain program's by a relative error of at most 0.019.
Values may be sent and summed in bfloat16 or wider, within the bound.
A program may use at most 64 MiB of HBM per device.

v0:
```python
import jax
import jax.numpy as jnp
from jax import lax
from jax.sharding import PartitionSpec as P

epsilon = 1e-06


def per_device(tokens, norm_gain, expert_ids, route_weights, w_gate, w_up, w_down):
    tok_rows, model_width = tokens.shape
    local_count = w_gate.shape[0]
    experts = local_count * lax.axis_size("ep")
    rank_count = lax.axis_size("tp")
    column_width = model_width // rank_count
    capacity = 4 * tok_rows // experts
    as_float = tokens.astype(jnp.float32)
    scale = lax.rsqrt(jnp.mean(as_float * as_float, axis=-1, keepdims=True) + epsilon)
    normed = (as_float * scale * norm_gain[None, :]).astype(jnp.bfloat16)
    flat_ids = expert_ids.reshape(-1)
    one_hot = (flat_ids[:, None] == jnp.arange(experts, dtype=jnp.int32)[None, :]).astype(jnp.int32)
    slot_index = jnp.sum((jnp.cumsum(one_hot, axis=0) - one_hot) * one_hot, axis=1)
    target = flat_ids * capacity + slot_index
    token_rows = jnp.repeat(normed, 2, axis=0)
    token_rows = lax.dynamic_slice_in_dim(
        token_rows, lax.axis_index("tp") * column_width, column_width, 1
    )
    outgoing = (
        jnp.zeros((experts * capacity, token_rows.shape[1]), jnp.bfloat16)
        .at[target]
        .set(token_rows)
    )
    outgoing = outgoing.reshape(experts, capacity, token_rows.shape[1])
    arrived = lax.all_to_all(outgoing, "ep", split_axis=0, concat_axis=1, tiled=True)
    piece = lax.all_gather(arrived, "tp", axis=2, tiled=True)
    gate_part = jnp.einsum("erd,edf->erf", piece, w_gate, preferred_element_type=jnp.float32)
    up_part = jnp.einsum("erd,edf->erf", piece, w_up, preferred_element_type=jnp.float32)
    hidden = (jax.nn.silu(gate_part) * up_part).astype(jnp.bfloat16)
    partial_value = jnp.einsum("erf,efd->erd", hidden, w_down, preferred_element_type=jnp.float32)
    summed = lax.psum_scatter(
        partial_value.astype(jnp.bfloat16), "tp", scatter_dimension=2, tiled=True
    )
    returned = lax.all_to_all(summed, "ep", split_axis=1, concat_axis=0, tiled=True)
    picked = returned.reshape(experts * capacity, column_width)[target]
    picked = picked.reshape(tok_rows, 2, column_width).astype(jnp.float32)
    return jnp.sum(picked * route_weights[:, :, None], axis=1).astype(jnp.bfloat16)


def solution(mesh):
    in_specs = (
        P("ep", None),
        P(),
        P("ep", None),
        P("ep", None),
        P("ep", None, "tp"),
        P("ep", None, "tp"),
        P("ep", "tp", None),
    )
    out_specs = P("ep", "tp")
    return jax.shard_map(
        per_device, mesh=mesh, in_specs=in_specs, out_specs=out_specs, check_vma=False
    )
```

profile of v0, /device:TPU:0, one launch (start us, length us, event | category | flops | bytes accessed | tf_op | source)
XLA Modules:
  0.0 143.9 jit_solution(12117852993632384072)
XLA Ops:
  6.5 0.8 copy.19
  7.6 0.7 broadcast_multiply_fusion
  8.3 0.6 reduce-window.6
  9.4 1.2 fusion.18
  10.6 1.2 fusion.20
  11.9 0.6 broadcast_in_dim.5
  12.5 0.4 reshape.102
  13.0 1.7 %scatter_custom_fusion = bf16[512,512]{1,0:T(8,128)(2,1)S(1)} fusion(s32[256]{0:T(256)S(1)} %bitcast.52, bf16[256,2048]{1,0:T(8,128)(2,1)S(1)} %reshape.102, s32[]{:T(128)} %constant.12.clone.1, s32[]{:T(128)S(6)} %select_n.15, bf16[]{:T(256)} %constant.10.clone.1), kind=kCustom, calls=%fused_computation.20 | custom fusion | bytes 786442 | tf_op jit(solution)/shard_map/scatter | solution.py:30
  14.7 21.7 %all_to_all.21 = bf16[8,64,512]{2,1,0:T(8,128)(2,1)} all-to-all(bf16[8,64,512]{2,1,0:T(8,128)(2,1)S(1)} %bitcast.51), channel_id=1, replica_groups=mesh['ep'=8,'tp'=4] {'ep'}, dimensions={0} | all-to-all | bytes 1048576 | tf_op jit(solution)/shard_map/all_to_all | solution.py:33
  36.5 0.2 reduce-scatter.2.cloned.1.call-start
  36.7 21.5 %all-gather.2.cloned.1.call-done = bf16[1,512,2048]{2,1,0:T(8,128)(2,1)} async-done(((bf16[1,512,512]{2,1,0:T(8,128)(2,1)}), bf16[1,512,2048]{2,1,0:T(8,128)(2,1)}) %all-gather.2.cloned.1.call-update) | async-done | bytes 2097168 | tf_op jit(solution)/shard_map/all_gather | solution.py:34
  58.2 6.6 %fusion.4 = f32[512,1024]{1,0:T(8,128)} fusion(bf16[1,2048,1024]{2,1,0:T(8,128)(2,1)} %param.11, bf16[1,512,2048]{2,1,0:T(8,128)(2,1)} %all-gather.2.cloned.1.call-done), kind=kOutput, calls=%fused_computation.6 | convolution fusion | flops 2147483648 | bytes 8388608 | tf_op jit(solution)/shard_map/erd,edf->erf/dot_general | solution.py:35
  64.8 10.0 %fusion.9 = bf16[1,512,2048]{2,1,0:T(8,128)(2,1)} fusion(bf16[1,1024,2048]{2,1,0:T(8,128)(2,1)} %param.13, f32[512,1024]{1,0:T(8,128)} %fusion.4, bf16[1,2048,1024]{2,1,0:T(8,128)(2,1)} %param.12, bf16[1,512,2048]{2,1,0:T(8,128)(2,1)S(1)} %copy-done.1), kind=kOutput, calls=%fused_computation.9 | convolution fusion | flops 4299161600 | bytes 14680064 | tf_op jit(solution)/shard_map/erf,efd->erd/dot_general | solution.py:38
  74.8 31.3 %reduce-scatter.2.cloned.1.call-done = bf16[1,512,512]{2,1,0:T(8,128)(2,1)} async-done(((bf16[1,512,2048]{2,1,0:T(8,128)(2,1)}), bf16[1,512,512]{2,1,0:T(8,128)(2,1)}) %reduce-scatter.2.cloned.1.call-update) | async-done | bytes 524304 | tf_op jit(solution)/shard_map/reduce_scatter | solution.py:39
  106.2 1.9 %copy.27 = bf16[1,512,512]{2,0,1:T(2,128)(2,1)S(1)} copy(bf16[1,512,512]{2,1,0:T(8,128)(2,1)} %reduce-scatter.2.cloned.1.call-done) | data formatting | bytes 1048576 | tf_op jit(solution)/shard_map/reduce_scatter | solution.py:39
  108.0 0.5 broadcast.73
  108.5 4.0 %reduce.2 = bf16[512,512]{1,0:T(8,128)(2,1)S(1)} reduce(bf16[512,1,512]{2,1,0:T(2,128)(2,1)S(1)} %bitcast.49, bf16[]{:T(256)} %broadcast.73), dimensions={1}, to_apply=%bitcast.46.reduce_sub_computation | reduce | bytes 1048578
  112.5 1.2 reshape.129
  113.7 5.5 %all-to-all-start.1 = ((bf16[8,2,16384]{2,1,0:T(2,128)(2,1)}), bf16[8,2,16384]{2,1,0:T(2,128)(2,1)S(1)}, u32[]{:S(2)}, u32[]{:S(2)}) async-start(bf16[8,2,16384]{2,1,0:T(2,128)(2,1)} %reshape.129), calls=%async_computation.2 | async-start | bytes 1048576 | tf_op jit(solution)/shard_map/all_to_all | solution.py:42
  119.3 14.2 %all-to-all-done.1 = bf16[8,2,16384]{2,1,0:T(2,128)(2,1)S(1)} async-done(((bf16[8,2,16384]{2,1,0:T(2,128)(2,1)}), bf16[8,2,16384]{2,1,0:T(2,128)(2,1)S(1)}, u32[]{:S(2)}, u32[]{:S(2)}) %all-to-all-start.1) | async-done | bytes 524320 | tf_op jit(solution)/shard_map/all_to_all | solution.py:42
  133.5 0.5 reshape.130
  134.2 1.2 gather_fusion
  135.3 0.3 reshape.109
  135.7 1.4 multiply_reduce_fusion
  (21 shorter events, 1.2 us)
Async XLA Ops:
  6.5 51.7 %all-gather.2.cloned.1.call-start = ((), (), s32[]{:S(2)}) async-start(), calls=%async_computation.3 | async-start | bytes 2621440 | tf_op jit(solution)/shard_map/all_gather | solution.py:34
  36.5 69.7 %reduce-scatter.2.cloned.1.call-start = ((), (), s32[]{:S(2)}) async-start(), calls=%async_computation.4 | async-start | bytes 2621440 | tf_op jit(solution)/shard_map/reduce_scatter | solution.py:39
  58.2 6.6 %copy-start.1 = (bf16[1,512,2048]{2,1,0:T(8,128)(2,1)S(1)}, bf16[1,512,2048]{2,1,0:T(8,128)(2,1)}, u32[]{:S(2)}) copy-start(bf16[1,512,2048]{2,1,0:T(8,128)(2,1)} %all-gather.2.cloned.1.call-done) | copy-start | bytes 6291460
  108.0 11.2 %copy-start = (f32[128,2]{0,1:T(2,128)S(1)}, f32[128,2]{0,1:T(2,128)}, u32[]{:S(2)}) copy-start(f32[128,2]{0,1:T(2,128)} %param.10) | copy-start | bytes 3076
  113.7 19.8 %all-to-all-start.1 = ((bf16[8,2,16384]{2,1,0:T(2,128)(2,1)}), bf16[8,2,16384]{2,1,0:T(2,128)(2,1)S(1)}, u32[]{:S(2)}, u32[]{:S(2)}) async-start(bf16[8,2,16384]{2,1,0:T(2,128)(2,1)} %reshape.129), calls=%async_computation.2 | async-start | bytes 1048576 | tf_op jit(solution)/shard_map/all_to_all | solution.py:42
Sparse Core Ops, SparseCore 0:
  36.6 21.5 all-gather.1
  75.0 31.1 reduce-scatter.1
where the time goes:
time: 144 us
  waiting for transfers between devices  67.1 us (47%)
  blocking collectives  21.7 us (15%)
  matrix products  16.6 us (12%)
  between operations  13.5 us (9%)
  local copies, waits for them, and re-layouts  10.1 us (7%)
  other arithmetic  9.19 us (6%)
  starting transfers between devices  5.74 us (4%)
    reduce_scatter x1, waiting for transfers between devices, per_device(): lax.psum_scatter(partial_value.astype(jnp.bfloat16), 'tp', scatter_dimens...  31.3 us
    all_to_all x1, blocking collectives, per_device(): lax.all_to_all(outgoing, 'ep', split_axis=0, concat_axis=1, tiled=True)  21.7 us
    all_gather x1, waiting for transfers between devices, per_device(): piece = lax.all_gather(arrived, 'tp', axis=2, tiled=True)  21.5 us
    all_to_all x1, waiting for transfers between devices, per_device(): lax.all_to_all(summed, 'ep', split_axis=1, concat_axis=0, tiled=True)  14.2 us
    dot_general x1, matrix products, per_device(): jnp.einsum('erf,efd->erd', hidden, w_down, preferred_element_type=jnp.flo...  9.99 us
    dot_general x1, matrix products, per_device(): jnp.einsum('erd,edf->erf', piece, w_gate, preferred_element_type=jnp.floa...  6.59 us
    all_to_all x1, starting transfers between devices, per_device(): lax.all_to_all(summed, 'ep', split_axis=1, concat_axis=0, tiled=True)  5.51 us
    unnamed x1, other arithmetic  3.95 us
  transfers between devices with their start and end apart: 3, of which 3 were waited for; matrix products, arithmetic and copies ran while one was open for 0% of the time, Pallas kernels for 0%

commit v1 on v0

v1 whole, which is shorter than its diff:
```python
import functools
import jax
import jax.numpy as jnp
from jax import lax
from jax.experimental import pallas as pl
from jax.experimental.pallas import tpu as pltpu
from jax.sharding import PartitionSpec as P

epsilon = 1e-06
MESH = pl.DeviceIdType.MESH
f32 = jnp.float32
bf16 = jnp.bfloat16


def kernel(n, tp, cap, tok_ref, gain_ref, ids_ref, rw_ref, wg_hbm, wu_hbm, wd_hbm, out_ref,
           wg, wu, wd, normed, send, xbuf, hid, part, rs1, s1, rs2, s2, ret, whi, wlo,
           w_sem, d_send, d_recv, y_send, y_recv, c_send, c_recv,
           p_send, p_recv, q_send, q_recv, r_send, r_recv):
    tok, width = tok_ref.shape
    ff = wg.shape[1]
    ny = tp // 2
    w = width // tp
    power = n & (n - 1) == 0
    half = n // 2
    me = lax.axis_index("ep")
    t = lax.axis_index("tp")
    core = lax.rem(t, 2)
    y = lax.div(t, 2)
    mate = y * 2 + 1 - core

    order = [0, 4, 1, 5, 2, 6, 3, 7] if n == 8 else None

    def shift(i, sign):
        if power:
            s = order[i] if order else i
            v, bit = me, 1
            while bit < n:
                if s & bit:
                    v = v + bit - 2 * bit * lax.rem(lax.div(v, bit), 2)
                bit *= 2
            return v
        return lax.rem(me + sign * i + n, n)

    def each(lo, hi, body):
        if power:
            for i in range(lo, hi):
                body(i)
        else:
            lax.fori_loop(lo, hi, lambda i, c: (body(i), c)[1], 0)

    def rows(i):
        return pl.ds(i * cap if isinstance(i, int) else pl.multiple_of(i * cap, cap), cap)

    def cols(p):
        return pl.ds(p * w if isinstance(p, int) else pl.multiple_of(p * w, w), w)

    def remote(src, dst, ss, rs, **where):
        return pltpu.make_async_remote_copy(
            src_ref=src, dst_ref=dst, send_sem=ss, recv_sem=rs,
            device_id=where, device_id_type=MESH)

    def y_peer(dy, sign=1):
        return lax.rem(y + sign * dy + ny, ny)

    def dispatch(i):
        e = shift(i, 1)
        return remote(send.at[rows(e)], xbuf.at[rows(i), cols(t)],
                      d_send.at[i], d_recv.at[i], ep=e)

    def y_copy(i, dy):
        at = xbuf.at[rows(i), cols(t)]
        return remote(at, at, y_send.at[i, dy], y_recv.at[i, dy], tp=y_peer(dy) * 2 + core)

    def y_wait(i, dy):
        at = xbuf.at[rows(i), cols(y_peer(dy, -1) * 2 + core)]
        remote(at, at, y_send.at[i, dy], y_recv.at[i, dy], tp=y_peer(dy) * 2 + core).wait_recv()

    def c_copy(i, dy):
        at = xbuf.at[rows(i), cols(y_peer(dy, -1) * 2 + core)]
        return remote(at, at, c_send.at[i, dy], c_recv.at[i, dy], tp=mate)

    def c_wait(i, dy):
        at = xbuf.at[rows(i), cols(y_peer(dy, -1) * 2 + 1 - core)]
        remote(at, at, c_send.at[i, dy], c_recv.at[i, dy], tp=mate).wait_recv()

    loads = [pltpu.make_async_copy(a.at[0], b, w_sem.at[k])
             for k, (a, b) in enumerate(((wg_hbm, wg), (wu_hbm, wu), (wd_hbm, wd)))]
    barrier = pltpu.get_barrier_semaphore()
    pl.semaphore_signal(barrier, inc=1, device_id={"tp": mate}, device_id_type=MESH)
    for dy in range(1, ny):
        pl.semaphore_signal(barrier, inc=1, device_id={"tp": y_peer(dy) * 2 + core},
                            device_id_type=MESH)
    each(1, n, lambda i: pl.semaphore_signal(
        barrier, inc=1, device_id={"ep": shift(i, 1)}, device_id_type=MESH))
    for load in loads:
        load.start()

    as_float = tok_ref[...].astype(f32)
    scale = lax.rsqrt(jnp.mean(as_float * as_float, axis=-1, keepdims=True) + epsilon)
    normed[...] = (as_float * scale * gain_ref[...]).astype(bf16)

    lanes = 128
    lane = lax.broadcasted_iota(jnp.int32, (tok, lanes), 1)
    first = ids_ref[:, 0:1] == lane
    second = ids_ref[:, 1:2] == lane
    named = (first | second).astype(f32).astype(bf16)
    weight = jnp.where(first, rw_ref[:, 0:1], 0.0) + jnp.where(second, rw_ref[:, 1:2], 0.0)
    earlier = (lax.broadcasted_iota(jnp.int32, (tok, tok), 1)
               < lax.broadcasted_iota(jnp.int32, (tok, tok), 0)).astype(f32).astype(bf16)
    before = jnp.dot(earlier, named, preferred_element_type=f32).astype(bf16)
    slots = n * cap
    j = lax.broadcasted_iota(jnp.int32, (lanes, slots), 1)
    spread = (lax.div(j, cap) == lax.broadcasted_iota(jnp.int32, (lanes, slots), 0))
    spread = spread.astype(f32).astype(bf16)
    at_slot = lax.rem(lax.broadcasted_iota(jnp.int32, (tok, slots), 1), cap).astype(f32)

    def spread_out(v):
        return jnp.dot(v, spread, preferred_element_type=f32)

    hit = jnp.where(spread_out(before) == at_slot, spread_out(named), 0.0)
    outgoing = lax.dot_general(hit.astype(bf16), normed[:, cols(t)],
                               (((0,), (0,)), ((), ())), preferred_element_type=f32)
    send[...] = outgoing.astype(bf16)

    pl.semaphore_wait(barrier, n - 1 + ny)
    each(1, n, lambda i: dispatch(i).start())

    mine = (lax.broadcasted_iota(jnp.int32, (lanes, cap), 0) == me).astype(f32).astype(bf16)
    own_slot = lax.broadcasted_iota(jnp.int32, (tok, cap), 1).astype(f32)
    own_hit = jnp.where(jnp.dot(before, mine, preferred_element_type=f32) == own_slot,
                        jnp.dot(named, mine, preferred_element_type=f32), 0.0)
    xbuf[0:cap, :] = lax.dot_general(own_hit.astype(bf16), normed[...],
                                     (((0,), (0,)), ((), ())),
                                     preferred_element_type=f32).astype(bf16)
    high = weight.astype(bf16)
    low = (weight - high.astype(f32)).astype(bf16)
    whi[...] = (hit * spread_out(high)).astype(bf16)
    wlo[...] = (hit * spread_out(low)).astype(bf16)

    def relay_first(lo, hi):
        def body(i):
            dispatch(i).wait_recv()
            for dy in range(1, ny):
                y_copy(i, dy).start()
            c_copy(i, 0).start()
        each(lo, hi, body)

    def relay_second(lo, hi):
        def body(i):
            for dy in range(1, ny):
                y_wait(i, dy)
                c_copy(i, dy).start()
        each(lo, hi, body)

    def settle(lo, hi):
        def body(i):
            for dy in range(ny):
                c_wait(i, dy)
        each(lo, hi, body)

    tile = min(256, ff)
    dtile = min(512, width)
    chunk = [pl.ds(0, half * cap), pl.ds(half * cap, (n - half) * cap)]

    def up(k):
        def step(f, c):
            at = pl.ds(pl.multiple_of(f * tile, tile), tile)
            x = xbuf[chunk[k], :]
            g = jnp.dot(x, wg[:, at], preferred_element_type=f32)
            u = jnp.dot(x, wu[:, at], preferred_element_type=f32)
            hid[chunk[k], at] = (g / (1.0 + jnp.exp(-g)) * u).astype(bf16)
            return c
        lax.fori_loop(0, ff // tile, step, 0)

    def down(k):
        def step(d, c):
            at = pl.ds(pl.multiple_of(d * dtile, dtile), dtile)
            part[chunk[k], at] = jnp.dot(hid[chunk[k], :], wd[:, at],
                                         preferred_element_type=f32).astype(bf16)
            return c
        lax.fori_loop(0, width // dtile, step, 0)

    def pair(k, v):
        return remote(part.at[chunk[k], cols(v * 2 + 1 - core)], rs1.at[chunk[k], cols(v)],
                      p_send.at[k, v], p_recv.at[k, v], tp=mate)

    def cross(k, dy):
        return remote(s1.at[chunk[k], cols(y_peer(dy))], rs2.at[dy - 1, chunk[k], :],
                      q_send.at[k, dy], q_recv.at[k, dy], tp=y_peer(dy) * 2 + core)

    def add_pair(k):
        for dy in [*range(1, ny), 0]:
            v = y_peer(dy)
            pair(k, v).wait_recv()
            s1[chunk[k], cols(v)] = (part[chunk[k], cols(v * 2 + core)].astype(f32)
                                     + rs1[chunk[k], cols(v)].astype(f32)).astype(bf16)
            if dy:
                cross(k, dy).start()

    def back(i):
        return remote(s2.at[rows(i)], ret.at[rows(me)], r_send.at[i], r_recv.at[i],
                      ep=shift(i, -1))

    def back_wait(i):
        e = shift(i, 1)
        remote(s2.at[rows(i)], ret.at[rows(e)], r_send.at[i], r_recv.at[i], ep=e).wait_recv()

    def add_cross(k):
        total = s1[chunk[k], cols(y)].astype(f32)
        for dy in range(1, ny):
            cross(k, dy).wait_recv()
            total = total + rs2[dy - 1, chunk[k], :].astype(f32)
        s2[chunk[k], :] = total.astype(bf16)
        if k == 0:
            each(1, half, lambda i: back(i).start())
            ret[rows(me), :] = s2[0:cap, :]
        else:
            each(half, n, lambda i: back(i).start())

    relay_first(1, half)
    relay_second(1, half)
    relay_first(half, n)
    settle(1, half)
    loads[0].wait()
    loads[1].wait()
    up(0)
    loads[2].wait()
    down(0)
    for v in range(ny):
        pair(0, v).start()
    relay_second(half, n)
    settle(half, n)
    add_pair(0)
    up(1)
    add_cross(0)
    down(1)
    for v in range(ny):
        pair(1, v).start()
    add_pair(1)
    add_cross(1)
    each(1, n, back_wait)
    out_ref[...] = (jnp.dot(whi[...], ret[...], preferred_element_type=f32)
                    + jnp.dot(wlo[...], ret[...], preferred_element_type=f32)).astype(bf16)

    def drain(i):
        dispatch(i).wait_send()
        for dy in range(1, ny):
            y_copy(i, dy).wait_send()
        for dy in range(ny):
            c_copy(i, dy).wait_send()
        back(i).wait_send()
    each(1, n, drain)
    for k in range(2):
        for v in range(ny):
            pair(k, v).wait_send()
        for dy in range(1, ny):
            cross(k, dy).wait_send()


def per_device(tokens, norm_gain, expert_ids, route_weights, w_gate, w_up, w_down):
    tok, width = tokens.shape
    n = lax.axis_size("ep")
    tp = lax.axis_size("tp")
    ff = w_gate.shape[2]
    experts = n * w_gate.shape[0]
    cap = -(-(4 * tok // experts) // 16) * 16
    w = width // tp
    ny = tp // 2
    r = n * cap
    dma = pltpu.SemaphoreType.DMA
    vmem = pl.BlockSpec(memory_space=pltpu.VMEM)
    anywhere = pl.BlockSpec(memory_space=pl.ANY)
    flops = 6 * r * width * ff
    return pl.pallas_call(
        functools.partial(kernel, n, tp, cap),
        out_shape=jax.ShapeDtypeStruct((tok, w), bf16),
        in_specs=[vmem] * 4 + [anywhere] * 3,
        out_specs=vmem,
        scratch_shapes=[
            pltpu.VMEM((width, ff), bf16),
            pltpu.VMEM((width, ff), bf16),
            pltpu.VMEM((ff, width), bf16),
            pltpu.VMEM((tok, width), bf16),
            pltpu.VMEM((r, w), bf16),
            pltpu.VMEM((r, width), bf16),
            pltpu.VMEM((r, ff), bf16),
            pltpu.VMEM((r, width), bf16),
            pltpu.VMEM((r, ny * w), bf16),
            pltpu.VMEM((r, ny * w), bf16),
            pltpu.VMEM((ny - 1, r, w), bf16),
            pltpu.VMEM((r, w), bf16),
            pltpu.VMEM((r, w), bf16),
            pltpu.VMEM((tok, r), bf16),
            pltpu.VMEM((tok, r), bf16),
            dma((3,)),
            dma((n,)), dma((n,)),
            dma((n, ny)), dma((n, ny)),
            dma((n, ny)), dma((n, ny)),
            dma((2, ny)), dma((2, ny)),
            dma((2, ny)), dma((2, ny)),
            dma((n,)), dma((n,)),
        ],
        compiler_params=pltpu.CompilerParams(
            collective_id=0, has_side_effects=True, vmem_limit_bytes=60 * 1024 * 1024),
        cost_estimate=pl.CostEstimate(
            flops=flops, bytes_accessed=6 * width * ff, transcendentals=r * ff),
    )(tokens, norm_gain.reshape(1, -1), expert_ids, route_weights, w_gate, w_up, w_down)


def solution(mesh):
    in_specs = (
        P("ep", None),
        P(),
        P("ep", None),
        P("ep", None),
        P("ep", None, "tp"),
        P("ep", None, "tp"),
        P("ep", "tp", None),
    )
    out_specs = P("ep", "tp")
    return jax.shard_map(
        per_device, mesh=mesh, in_specs=in_specs, out_specs=out_specs, check_vma=False
    )
```

time: 144 us -> 62.2 us (0.43)
  waiting for transfers between devices: 67.1 us -> 0 us
  Pallas kernels: 0 us -> 57.6 us
  blocking collectives: 21.7 us -> 0 us
  matrix products: 16.6 us -> 0 us
  between operations: 13.5 us -> 0.01 us
  other arithmetic: 9.19 us -> 0 us
  starting transfers between devices: 5.74 us -> 0 us
  local copies, waits for them, and re-layouts: 10.1 us -> 4.38 us
    pallas_call x0 -> x1, Pallas kernels: none -> 57.6 us  [per_device(): pl.pallas_call(functools.partial(kernel, n, tp, cap), out_shape=jax.Shape...]
    reduce_scatter x1 -> x0, waiting for transfers between devices: 31.3 us -> none  [per_device(): lax.psum_scatter(partial_value.astype(jnp.bfloat16), 'tp', scatter_dimens...]
    all_to_all x1 -> x0, blocking collectives: 21.7 us -> none  [per_device(): lax.all_to_all(outgoing, 'ep', split_axis=0, concat_axis=1, tiled=True)]
    all_gather x1 -> x0, waiting for transfers between devices: 21.5 us -> none  [per_device(): piece = lax.all_gather(arrived, 'tp', axis=2, tiled=True)]
    dot_general x2 -> x0, matrix products: 16.6 us -> none  [the longest x1 9.99 us: per_device(): jnp.einsum('erf,efd->erd', hidden, w_down, preferred_element_type=jnp.flo...]
    all_to_all x1 -> x0, waiting for transfers between devices: 14.2 us -> none  [per_device(): lax.all_to_all(summed, 'ep', split_axis=1, concat_axis=0, tiled=True)]
    all_to_all x1 -> x0, starting transfers between devices: 5.51 us -> none  [per_device(): lax.all_to_all(summed, 'ep', split_axis=1, concat_axis=0, tiled=True)]
    unnamed x1 -> x0, other arithmetic: 3.95 us -> none
  transfers between devices with their start and end apart: 3 -> 0, of which waited for: 3 -> 0; matrix products, arithmetic and copies ran while one was open for 0% -> 0% of each run, Pallas kernels for 0% -> 0%
where the time goes in v1:
time: 62.2 us; the launch traced here: 62 us
  Pallas kernels  57.6 us (93%)
  local copies, waits for them, and re-layouts  4.38 us (7%)
    pallas_call x1, Pallas kernels, per_device(): pl.pallas_call(functools.partial(kernel, n, tp, cap), out_shape=jax.Shape...  57.6 us
    unnamed x3, local copies, waits for them, and re-layouts  4.38 us

profile of v1, /device:TPU:0, one launch (start us, length us, event | category | flops | bytes accessed | tf_op | source)
XLA Modules:
  0.0 62.0 jit_solution(16595113363522611515)
XLA Ops:
  0.0 1.4 %copy.8.ids_ref = s32[128,2]{1,0:T(8,128)} copy(s32[128,2]{0,1:T(2,128)} %param.9) | data formatting | bytes 2048 | tf_op args[2]
  1.4 1.4 %copy.9.rw_ref = f32[128,2]{1,0:T(8,128)} copy(f32[128,2]{0,1:T(2,128)} %param.10) | data formatting | bytes 2048 | tf_op args[3]
  2.8 57.6 %shard_map.73 = bf16[128,512]{1,0:T(8,128)(2,1)} custom-call(bf16[128,2048]{1,0:T(8,128)(2,1)} %tok_ref.1, f32[1,2048]{1,0:T(1,128)} %bitcast.1, s32[128,2]{1,0:T(8,128)} %copy.8.ids_ref, f32[128,2]{1,0:T(8,128)} %copy.9.rw_ref, bf16[1,2048,1024]{2,1,0:T(8,128)(2,1)} %wg_hbm.1, bf16[1,2048,1024]{2,1,0:T(8,128)(2,1)} %wu_hbm.1, bf16[1,1024,2048]{2,1,0:T(8,128)(2,1)} %wd_hbm.1), custom_call_target="tpu_custom_call" | custom-call | flops 6442450944 | bytes 12582912 | tf_op jit(solution)/shard_map/pallas_call | solution.py:274
  60.4 1.6 %copy.11 = bf16[128,512]{1,0:T(8,128)(2,1)} copy(bf16[128,512]{1,0:T(8,128)(2,1)} %shard_map.73) | data formatting | bytes 262144

commit v2 on v1

--- a/solution.py
+++ b/solution.py
@@ -28,7 +28,7 @@
     y = lax.div(t, 2)
     mate = y * 2 + 1 - core
 
-    order = [0, 4, 1, 5, 2, 6, 3, 7] if n == 8 else None
+    order = [0, 1, 2, 4, 3, 5, 6, 7] if n == 8 else None
 
     def shift(i, sign):
         if power:
@@ -99,43 +99,34 @@
     scale = lax.rsqrt(jnp.mean(as_float * as_float, axis=-1, keepdims=True) + epsilon)
     normed[...] = (as_float * scale * gain_ref[...]).astype(bf16)
 
-    lanes = 128
-    lane = lax.broadcasted_iota(jnp.int32, (tok, lanes), 1)
-    first = ids_ref[:, 0:1] == lane
-    second = ids_ref[:, 1:2] == lane
-    named = (first | second).astype(f32).astype(bf16)
-    weight = jnp.where(first, rw_ref[:, 0:1], 0.0) + jnp.where(second, rw_ref[:, 1:2], 0.0)
-    earlier = (lax.broadcasted_iota(jnp.int32, (tok, tok), 1)
-               < lax.broadcasted_iota(jnp.int32, (tok, tok), 0)).astype(f32).astype(bf16)
-    before = jnp.dot(earlier, named, preferred_element_type=f32).astype(bf16)
     slots = n * cap
-    j = lax.broadcasted_iota(jnp.int32, (lanes, slots), 1)
-    spread = (lax.div(j, cap) == lax.broadcasted_iota(jnp.int32, (lanes, slots), 0))
-    spread = spread.astype(f32).astype(bf16)
-    at_slot = lax.rem(lax.broadcasted_iota(jnp.int32, (tok, slots), 1), cap).astype(f32)
-
-    def spread_out(v):
-        return jnp.dot(v, spread, preferred_element_type=f32)
-
-    hit = jnp.where(spread_out(before) == at_slot, spread_out(named), 0.0)
-    outgoing = lax.dot_general(hit.astype(bf16), normed[:, cols(t)],
-                               (((0,), (0,)), ((), ())), preferred_element_type=f32)
-    send[...] = outgoing.astype(bf16)
+    experts = 128
+    first, second = ids_ref[0:1, :], ids_ref[1:2, :]
+    expert = lax.broadcasted_iota(jnp.int32, (experts, tok), 0)
+    is_first, is_second = first == expert, second == expert
+    named = (is_first | is_second).astype(f32).astype(bf16)
+    earlier = (lax.broadcasted_iota(jnp.int32, (tok, tok), 0)
+               < lax.broadcasted_iota(jnp.int32, (tok, tok), 1)).astype(f32).astype(bf16)
+    before = jnp.dot(named, earlier, preferred_element_type=f32)
+    place1 = first * cap + jnp.sum(jnp.where(is_first, before, 0.0), axis=0,
+                                   keepdims=True).astype(jnp.int32)
+    place2 = second * cap + jnp.sum(jnp.where(is_second, before, 0.0), axis=0,
+                                    keepdims=True).astype(jnp.int32)
+    slot = lax.broadcasted_iota(jnp.int32, (slots, tok), 0)
+    hit1, hit2 = slot == place1, slot == place2
+    send[...] = jnp.dot((hit1 | hit2).astype(f32).astype(bf16), normed[:, cols(t)],
+                        preferred_element_type=f32).astype(bf16)
 
     pl.semaphore_wait(barrier, n - 1 + ny)
     each(1, n, lambda i: dispatch(i).start())
 
-    mine = (lax.broadcasted_iota(jnp.int32, (lanes, cap), 0) == me).astype(f32).astype(bf16)
-    own_slot = lax.broadcasted_iota(jnp.int32, (tok, cap), 1).astype(f32)
-    own_hit = jnp.where(jnp.dot(before, mine, preferred_element_type=f32) == own_slot,
-                        jnp.dot(named, mine, preferred_element_type=f32), 0.0)
-    xbuf[0:cap, :] = lax.dot_general(own_hit.astype(bf16), normed[...],
-                                     (((0,), (0,)), ((), ())),
-                                     preferred_element_type=f32).astype(bf16)
+    own = lax.broadcasted_iota(jnp.int32, (cap, tok), 0) + me * cap
+    own_hit = ((own == place1) | (own == place2)).astype(f32).astype(bf16)
+    xbuf[0:cap, :] = jnp.dot(own_hit, normed[...], preferred_element_type=f32).astype(bf16)
+    weight = (jnp.where(hit1, rw_ref[0:1, :], 0.0) + jnp.where(hit2, rw_ref[1:2, :], 0.0)).T
     high = weight.astype(bf16)
-    low = (weight - high.astype(f32)).astype(bf16)
-    whi[...] = (hit * spread_out(high)).astype(bf16)
-    wlo[...] = (hit * spread_out(low)).astype(bf16)
+    whi[...] = high
+    wlo[...] = (weight - high.astype(f32)).astype(bf16)
 
     def relay_first(lo, hi):
         def body(i):
@@ -159,10 +150,9 @@
         each(lo, hi, body)
 
     tile = min(256, ff)
-    dtile = min(512, width)
     chunk = [pl.ds(0, half * cap), pl.ds(half * cap, (n - half) * cap)]
 
-    def up(k):
+    def up(k, lo, hi):
         def step(f, c):
             at = pl.ds(pl.multiple_of(f * tile, tile), tile)
             x = xbuf[chunk[k], :]
@@ -170,23 +160,23 @@
             u = jnp.dot(x, wu[:, at], preferred_element_type=f32)
             hid[chunk[k], at] = (g / (1.0 + jnp.exp(-g)) * u).astype(bf16)
             return c
-        lax.fori_loop(0, ff // tile, step, 0)
-
-    def down(k):
-        def step(d, c):
-            at = pl.ds(pl.multiple_of(d * dtile, dtile), dtile)
+        lax.fori_loop(lo, hi, step, 0)
+
+    def down(k, c):
+        def step(v, carry):
+            at = cols(v * 2 + c)
             part[chunk[k], at] = jnp.dot(hid[chunk[k], :], wd[:, at],
                                          preferred_element_type=f32).astype(bf16)
-            return c
-        lax.fori_loop(0, width // dtile, step, 0)
+            return carry
+        lax.fori_loop(0, ny, step, 0)
 
     def pair(k, v):
         return remote(part.at[chunk[k], cols(v * 2 + 1 - core)], rs1.at[chunk[k], cols(v)],
                       p_send.at[k, v], p_recv.at[k, v], tp=mate)
 
-    def cross(k, dy):
-        return remote(s1.at[chunk[k], cols(y_peer(dy))], rs2.at[dy - 1, chunk[k], :],
-                      q_send.at[k, dy], q_recv.at[k, dy], tp=y_peer(dy) * 2 + core)
+    def cross(i, dy):
+        return remote(s1.at[rows(i), cols(y_peer(dy))], rs2.at[dy - 1, rows(i), :],
+                      q_send.at[i, dy], q_recv.at[i, dy], tp=y_peer(dy) * 2 + core)
 
     def add_pair(k):
         for dy in [*range(1, ny), 0]:
@@ -195,7 +185,7 @@
             s1[chunk[k], cols(v)] = (part[chunk[k], cols(v * 2 + core)].astype(f32)
                                      + rs1[chunk[k], cols(v)].astype(f32)).astype(bf16)
             if dy:
-                cross(k, dy).start()
+                each(*span[k], lambda i: cross(i, dy).start())
 
     def back(i):
         return remote(s2.at[rows(i)], ret.at[rows(me)], r_send.at[i], r_recv.at[i],
@@ -205,39 +195,46 @@
         e = shift(i, 1)
         remote(s2.at[rows(i)], ret.at[rows(e)], r_send.at[i], r_recv.at[i], ep=e).wait_recv()
 
-    def add_cross(k):
-        total = s1[chunk[k], cols(y)].astype(f32)
+    def total(i):
+        value = s1[rows(i), cols(y)].astype(f32)
         for dy in range(1, ny):
-            cross(k, dy).wait_recv()
-            total = total + rs2[dy - 1, chunk[k], :].astype(f32)
-        s2[chunk[k], :] = total.astype(bf16)
-        if k == 0:
-            each(1, half, lambda i: back(i).start())
-            ret[rows(me), :] = s2[0:cap, :]
-        else:
-            each(half, n, lambda i: back(i).start())
-
-    relay_first(1, half)
+            cross(i, dy).wait_recv()
+            value = value + rs2[dy - 1, rows(i), :].astype(f32)
+        return value.astype(bf16)
+
+    def finish(lo, hi):
+        def body(i):
+            s2[rows(i), :] = total(i)
+            back(i).start()
+        each(lo, hi, body)
+
+    span = [(0, half), (half, n)]
+    tiles = ff // tile
+    relay_first(1, n)
     relay_second(1, half)
-    relay_first(half, n)
     settle(1, half)
     loads[0].wait()
     loads[1].wait()
-    up(0)
+    up(0, 0, tiles)
+    relay_second(half, n)
     loads[2].wait()
-    down(0)
+    down(0, 1 - core)
     for v in range(ny):
         pair(0, v).start()
-    relay_second(half, n)
+    down(0, core)
     settle(half, n)
+    up(1, 0, tiles // 2)
     add_pair(0)
-    up(1)
-    add_cross(0)
-    down(1)
+    up(1, tiles // 2, tiles)
+    finish(1, 2)
+    down(1, 1 - core)
     for v in range(ny):
         pair(1, v).start()
+    finish(2, half)
+    down(1, core)
     add_pair(1)
-    add_cross(1)
+    ret[rows(me), :] = total(0)
+    finish(half, n)
     each(1, n, back_wait)
     out_ref[...] = (jnp.dot(whi[...], ret[...], preferred_element_type=f32)
                     + jnp.dot(wlo[...], ret[...], preferred_element_type=f32)).astype(bf16)
@@ -250,11 +247,14 @@
             c_copy(i, dy).wait_send()
         back(i).wait_send()
     each(1, n, drain)
+
+    def drain_cross(i):
+        for dy in range(1, ny):
+            cross(i, dy).wait_send()
+    each(0, n, drain_cross)
     for k in range(2):
         for v in range(ny):
             pair(k, v).wait_send()
-        for dy in range(1, ny):
-            cross(k, dy).wait_send()
 
 
 def per_device(tokens, norm_gain, expert_ids, route_weights, w_gate, w_up, w_down):
@@ -297,14 +297,14 @@
             dma((n, ny)), dma((n, ny)),
             dma((n, ny)), dma((n, ny)),
             dma((2, ny)), dma((2, ny)),
-            dma((2, ny)), dma((2, ny)),
+            dma((n, ny)), dma((n, ny)),
             dma((n,)), dma((n,)),
         ],
         compiler_params=pltpu.CompilerParams(
             collective_id=0, has_side_effects=True, vmem_limit_bytes=60 * 1024 * 1024),
         cost_estimate=pl.CostEstimate(
             flops=flops, bytes_accessed=6 * width * ff, transcendentals=r * ff),
-    )(tokens, norm_gain.reshape(1, -1), expert_ids, route_weights, w_gate, w_up, w_down)
+    )(tokens, norm_gain.reshape(1, -1), expert_ids.T, route_weights.T, w_gate, w_up, w_down)
 
 
 def solution(mesh):

time: 62.2 us -> 52.7 us (0.85)
  Pallas kernels: 57.6 us -> 51 us
  local copies, waits for them, and re-layouts: 4.38 us -> 1.57 us
    pallas_call x1, Pallas kernels: 57.6 us -> 51 us  [per_device(): pl.pallas_call(functools.partial(kernel, n, tp, cap), out_shape=jax.Shape...]
    unnamed x3 -> x1, local copies, waits for them, and re-layouts: 4.38 us -> 1.57 us
where the time goes in v2:
time: 52.7 us; the launch traced here: 52.6 us
  Pallas kernels  51 us (97%)
  local copies, waits for them, and re-layouts  1.57 us (3%)
    pallas_call x1, Pallas kernels, per_device(): pl.pallas_call(functools.partial(kernel, n, tp, cap), out_shape=jax.Shape...  51 us
    unnamed x1, local copies, waits for them, and re-layouts  1.57 us

profile of v2, /device:TPU:0, one launch (start us, length us, event | category | flops | bytes accessed | tf_op | source)
XLA Modules:
  0.0 52.6 jit_solution(15718842003654029180)
XLA Ops:
  0.0 51.0 %shard_map.73 = bf16[128,512]{1,0:T(8,128)(2,1)} custom-call(bf16[128,2048]{1,0:T(8,128)(2,1)} %tok_ref.1, f32[1,2048]{1,0:T(1,128)} %bitcast.3, s32[2,128]{1,0:T(2,128)} %bitcast.4, f32[2,128]{1,0:T(2,128)} %bitcast.5, bf16[1,2048,1024]{2,1,0:T(8,128)(2,1)} %wg_hbm.1, bf16[1,2048,1024]{2,1,0:T(8,128)(2,1)} %wu_hbm.1, bf16[1,1024,2048]{2,1,0:T(8,128)(2,1)} %wd_hbm.1), custom_call_target="tpu_custom_call" | custom-call | flops 6442450944 | bytes 12582912 | tf_op jit(solution)/shard_map/pallas_call | solution.py:274
  51.0 1.6 %copy.9 = bf16[128,512]{1,0:T(8,128)(2,1)} copy(bf16[128,512]{1,0:T(8,128)(2,1)} %shard_map.73) | data formatting | bytes 262144

commit v3 on v2

--- a/solution.py
+++ b/solution.py
@@ -13,7 +13,7 @@
 
 
 def kernel(n, tp, cap, tok_ref, gain_ref, ids_ref, rw_ref, wg_hbm, wu_hbm, wd_hbm, out_ref,
-           wg, wu, wd, normed, send, xbuf, hid, part, rs1, s1, rs2, s2, ret, whi, wlo,
+           wg, wu, wd, normed, send, send2, xbuf, hid, part, rs1, s1, rs2, s2, ret, whi, wlo,
            w_sem, d_send, d_recv, y_send, y_recv, c_send, c_recv,
            p_send, p_recv, q_send, q_recv, r_send, r_recv):
     tok, width = tok_ref.shape
@@ -28,7 +28,9 @@
     y = lax.div(t, 2)
     mate = y * 2 + 1 - core
 
-    order = [0, 1, 2, 4, 3, 5, 6, 7] if n == 8 else None
+    order = [0, 1, 4, 5, 2, 3, 6, 7] if n == 8 else None
+    direct = [1, 4] if n == 8 and ny == 2 else []
+    cross_order = [[2, 3, 1, 0], [6, 7, 5, 4]] if n == 8 else None
 
     def shift(i, sign):
         if power:
@@ -120,6 +122,16 @@
     pl.semaphore_wait(barrier, n - 1 + ny)
     each(1, n, lambda i: dispatch(i).start())
 
+    for i in direct:
+        e = shift(i, 1)
+        row = lax.broadcasted_iota(jnp.int32, (cap, tok), 0) + e * cap
+        at_row = ((row == place1) | (row == place2)).astype(f32).astype(bf16)
+        other = cols(y_peer(1) * 2 + core)
+        send2[rows(i), :] = jnp.dot(at_row, normed[:, other],
+                                    preferred_element_type=f32).astype(bf16)
+        remote(send2.at[rows(i)], xbuf.at[rows(i), other],
+               y_send.at[i, 1], y_recv.at[i, 1], ep=e).start()
+
     own = lax.broadcasted_iota(jnp.int32, (cap, tok), 0) + me * cap
     own_hit = ((own == place1) | (own == place2)).astype(f32).astype(bf16)
     xbuf[0:cap, :] = jnp.dot(own_hit, normed[...], preferred_element_type=f32).astype(bf16)
@@ -132,7 +144,8 @@
         def body(i):
             dispatch(i).wait_recv()
             for dy in range(1, ny):
-                y_copy(i, dy).start()
+                if i not in direct:
+                    y_copy(i, dy).start()
             c_copy(i, 0).start()
         each(lo, hi, body)
 
@@ -185,7 +198,11 @@
             s1[chunk[k], cols(v)] = (part[chunk[k], cols(v * 2 + core)].astype(f32)
                                      + rs1[chunk[k], cols(v)].astype(f32)).astype(bf16)
             if dy:
-                each(*span[k], lambda i: cross(i, dy).start())
+                if cross_order:
+                    for i in cross_order[k]:
+                        cross(i, dy).start()
+                else:
+                    each(*span[k], lambda i: cross(i, dy).start())
 
     def back(i):
         return remote(s2.at[rows(i)], ret.at[rows(me)], r_send.at[i], r_recv.at[i],
@@ -202,11 +219,15 @@
             value = value + rs2[dy - 1, rows(i), :].astype(f32)
         return value.astype(bf16)
 
-    def finish(lo, hi):
+    def finish(k, lo, hi):
         def body(i):
             s2[rows(i), :] = total(i)
             back(i).start()
-        each(lo, hi, body)
+        if cross_order:
+            for i in [i for i in cross_order[k] if i][lo - k * half - (k == 0):hi - k * half - (k == 0)]:
+                body(i)
+        else:
+            each(lo, hi, body)
 
     span = [(0, half), (half, n)]
     tiles = ff // tile
@@ -222,19 +243,18 @@
     for v in range(ny):
         pair(0, v).start()
     down(0, core)
+    add_pair(0)
     settle(half, n)
-    up(1, 0, tiles // 2)
-    add_pair(0)
-    up(1, tiles // 2, tiles)
-    finish(1, 2)
+    up(1, 0, tiles)
+    finish(0, 1, 2)
     down(1, 1 - core)
     for v in range(ny):
         pair(1, v).start()
-    finish(2, half)
+    finish(0, 2, half)
     down(1, core)
     add_pair(1)
     ret[rows(me), :] = total(0)
-    finish(half, n)
+    finish(1, half, n)
     each(1, n, back_wait)
     out_ref[...] = (jnp.dot(whi[...], ret[...], preferred_element_type=f32)
                     + jnp.dot(wlo[...], ret[...], preferred_element_type=f32)).astype(bf16)
@@ -282,6 +302,7 @@
             pltpu.VMEM((ff, width), bf16),
             pltpu.VMEM((tok, width), bf16),
             pltpu.VMEM((r, w), bf16),
+            pltpu.VMEM((r, w), bf16),
             pltpu.VMEM((r, width), bf16),
             pltpu.VMEM((r, ff), bf16),
             pltpu.VMEM((r, width), bf16),

time: 52.7 us -> 48.9 us (0.928)
  Pallas kernels: 51 us -> 47.2 us
    pallas_call x1, Pallas kernels: 51 us -> 47.2 us  [per_device(): pl.pallas_call(functools.partial(kernel, n, tp, cap), out_shape=jax.Shape...]
where the time goes in v3:
time: 48.9 us; the launch traced here: 48.8 us
  Pallas kernels  47.2 us (97%)
  local copies, waits for them, and re-layouts  1.57 us (3%)
    pallas_call x1, Pallas kernels, per_device(): pl.pallas_call(functools.partial(kernel, n, tp, cap), out_shape=jax.Shape...  47.2 us
    unnamed x1, local copies, waits for them, and re-layouts  1.57 us

profile of v3, /device:TPU:0, one launch (start us, length us, event | category | flops | bytes accessed | tf_op | source)
XLA Modules:
  0.0 48.8 jit_solution(1003558164009969263)
XLA Ops:
  0.0 47.2 %shard_map.73 = bf16[128,512]{1,0:T(8,128)(2,1)} custom-call(bf16[128,2048]{1,0:T(8,128)(2,1)} %tok_ref.1, f32[1,2048]{1,0:T(1,128)} %bitcast.3, s32[2,128]{1,0:T(2,128)} %bitcast.4, f32[2,128]{1,0:T(2,128)} %bitcast.5, bf16[1,2048,1024]{2,1,0:T(8,128)(2,1)} %wg_hbm.1, bf16[1,2048,1024]{2,1,0:T(8,128)(2,1)} %wu_hbm.1, bf16[1,1024,2048]{2,1,0:T(8,128)(2,1)} %wd_hbm.1), custom_call_target="tpu_custom_call" | custom-call | flops 6442450944 | bytes 12582912 | tf_op jit(solution)/shard_map/pallas_call | solution.py:294
  47.2 1.6 %copy.9 = bf16[128,512]{1,0:T(8,128)(2,1)} copy(bf16[128,512]{1,0:T(8,128)(2,1)} %shard_map.73) | data formatting | bytes 262144
